TPU v7x, 32 devices: a whole 2x2x4 slice. The times are simulated.
32 devices in a mesh: grp: 2 (over y), ep: 8 (over z, core), tp: 2 (over x).
Axes of the slice: x: 2, y: 2, z: 4, core: 2. Of those that a mesh axis runs over, the one named last changes fastest.
Arguments:
- recurrence_query_input: bfloat16 [2048, 2048], P(('grp', 'ep'), 'tp'), parts along dimension 0, may hold values from -6 to 6
- forget_gate_input: bfloat16 [2048, 2048], P(('grp', 'ep'), 'tp'), parts along dimension 0, may hold values from -6.5 to 6.5
- recurrence_value_input: bfloat16 [2048, 2048], P(('grp', 'ep'), 'tp'), parts along dimension 0, may hold values from -6 to 6
- output_gate_input: bfloat16 [2048, 2048], P(('grp', 'ep'), 'tp'), parts along dimension 0, may hold values from -6 to 6
- forget_lower_margin: float32 [2048], P('tp'), may hold values from 0 to 0.1
- position_decay_extra: float32 [2048, 16], P(('grp', 'ep'), 'tp'), parts along dimension 0, may hold values from -2.1 to 0
- head_norm_gain: float32 [2048], P('tp'), may hold values from 0.1 to 1.9
- recurrence_out_weight: bfloat16 [2048, 2048], P('tp'), may hold values from -0.125 to 0.125
- expert_hidden_state: bfloat16 [2048, 2048], P(('grp', 'ep')), parts along dimension 0, may hold values from -6 to 6
- chosen_expert_index: int32 [2048, 4], P(('grp', 'ep')), parts along dimension 0, may hold values from 0 to 7, all different within a row; in each aligned block of 128 rows (0 to 127, 128 to 255, ...) at most 128 rows name the same one
- chosen_expert_score: float32 [2048, 4], P(('grp', 'ep')), parts along dimension 0, may hold values from 0.02 to 1
- expert_norm_gain: float32 [2048], replicated, may hold values from 0.1 to 1.9
- routed_gate_weight: bfloat16 [8, 2048, 1024], P('ep', None, 'tp'), may hold values from -0.125 to 0.125
- routed_up_weight: bfloat16 [8, 2048, 1024], P('ep', None, 'tp'), may hold values from -0.125 to 0.125
- routed_down_weight: bfloat16 [8, 1024, 2048], P('ep', None, 'tp'), may hold values from -0.1875 to 0.1875
- shared_gate_weight: bfloat16 [2048, 1024], P(None, 'tp'), may hold values from -0.125 to 0.125
- shared_up_weight: bfloat16 [2048, 1024], P(None, 'tp'), may hold values from -0.125 to 0.125
- shared_down_weight: bfloat16 [1024, 2048], P(None, 'tp'), may hold values from -0.1875 to 0.1875
Outputs:
- recurrence_output: bfloat16 [2048, 2048], P(('grp', 'ep', 'tp')), parts along dimension 0
- expert_out: bfloat16 [2048, 2048], P(('grp', 'ep'), 'tp'), parts along dimension 0
There are 2 independent parts, one for each index of `grp`. A program takes and returns all parts, laid end to end along the dimension named above; an argument that names none is the same for every part. Nothing has to cross between parts.
Inputs may be any that keep to these rules, and one draw needn't show every extreme that they name: `chosen_expert_index`: each row names 4 different experts. In each aligned block of 128 rows (the rows of one index of ep) no expert is named by more than 128 rows, and in every draw some block names some expert exactly 128 times.
All inputs are finite; a program needn't handle non-finite values.
Results may differ from a plain program's by a relative error of at most 0.015.
Values may be sent and summed in bfloat16 or wider, within the bound.
A program may use at most 64 MiB of HBM per device.

v0:
```python
import jax
import jax.numpy as jnp
from jax import lax
from jax.sharding import PartitionSpec as P

HEAD_CHANNELS = 128
BLK = 64
EPSILON = 1e-06
ROUTED_SCALE = 2.5
PRECISION = lax.Precision.DEFAULT


def carried_in(array, axis, combine, identity):
    count, index = (lax.axis_size(axis), lax.axis_index(axis))
    everything = jax.tree.map(
        lambda part, kind: lax.all_gather(part.astype(kind), axis),
        array,
        (jnp.bfloat16, jnp.bfloat16),
    )
    start = jax.tree.map(
        lambda part, zero: jnp.broadcast_to(jnp.asarray(zero, part.dtype), part.shape),
        array,
        identity,
    )

    def turn(k, before):
        reached = k < index
        new = combine(
            before, jax.tree.map(lambda part, own: part[k].astype(own.dtype), everything, array)
        )
        return jax.tree.map(lambda a, b: jnp.where(reached, a, b), new, before)

    return lax.fori_loop(0, count, turn, start)


def chain_states(earlier, later):
    return (earlier[0] * later[0], later[0][..., None] * earlier[1] + later[1])


def mixer_half(
    recurrence_query_input,
    forget_gate_input,
    recurrence_value_input,
    output_gate_input,
    forget_lower_margin,
    position_decay_extra,
    head_norm_gain,
    recurrence_out_weight,
):
    length = recurrence_query_input.shape[0]
    head_tensor = position_decay_extra.shape[1]
    blocks = length // BLK
    queries = jax.nn.silu(recurrence_query_input.astype(jnp.float32))
    key_gate_value = forget_lower_margin[None, :] * jax.nn.sigmoid(
        -forget_gate_input.astype(jnp.float32)
    )
    decay_logarithm = jnp.log1p(-key_gate_value) + jnp.repeat(
        position_decay_extra, HEAD_CHANNELS, axis=1
    )
    value_rows = recurrence_value_input.astype(jnp.float32)

    def split_heads(tensor):
        return tensor.reshape(blocks, BLK, head_tensor, HEAD_CHANNELS).transpose(2, 0, 1, 3)

    query_heads = split_heads(queries)
    key_heads = split_heads(key_gate_value)
    value_heads = split_heads(value_rows)
    cum_decay = jnp.cumsum(split_heads(decay_logarithm), axis=2)
    middle = cum_decay[:, :, BLK // 2 - 1 : BLK // 2]
    block_end = cum_decay[:, :, BLK - 1 : BLK]
    scores = jnp.einsum(
        "hncd,hnsd->hncs",
        query_heads * jnp.exp(cum_decay - middle),
        key_heads * jnp.exp(middle - cum_decay),
        precision=PRECISION,
    )
    causal = jnp.tril(jnp.ones((BLK, BLK), dtype=bool))
    scores = jnp.where(causal, scores, 0.0)
    within = jnp.einsum("hncs,hnse->hnce", scores, value_heads, precision=PRECISION)
    updates = jnp.einsum(
        "hncd,hnce->nhde",
        key_heads * jnp.exp(block_end - cum_decay),
        value_heads,
        precision=PRECISION,
    )
    block_log = block_end[:, :, 0, :]
    block_decay = jnp.exp(block_log).transpose(1, 0, 2)

    def advance(carry_state, inputs):
        factor, update = inputs
        return (factor[..., None] * carry_state + update, carry_state)

    initial = jnp.zeros((head_tensor, HEAD_CHANNELS, HEAD_CHANNELS), jnp.float32)
    local_final, local_starts = lax.scan(advance, initial, (block_decay, updates))
    device_decay = jnp.exp(jnp.sum(block_log, axis=1))
    identity = (jnp.ones_like(device_decay), jnp.zeros_like(local_final))
    _, incoming = carried_in((device_decay, local_final), "ep", chain_states, identity)
    before = jnp.exp(jnp.cumsum(block_log, axis=1) - block_log).transpose(1, 0, 2)
    starts = local_starts + before[..., None] * incoming[None]
    carried = jnp.einsum(
        "hncd,nhde->hnce", query_heads * jnp.exp(cum_decay), starts, precision=PRECISION
    )
    outputs = (within + carried).transpose(1, 2, 0, 3).reshape(length, head_tensor, HEAD_CHANNELS)
    factor = lax.rsqrt(jnp.mean(outputs * outputs, axis=2, keepdims=True) + EPSILON)
    normed = (outputs * factor).reshape(length, head_tensor * HEAD_CHANNELS) * head_norm_gain[
        None, :
    ]
    gated_rows = (normed * jax.nn.silu(output_gate_input.astype(jnp.float32))).astype(jnp.bfloat16)
    return lax.psum_scatter(
        jnp.dot(gated_rows, recurrence_out_weight, preferred_element_type=jnp.float32).astype(
            jnp.bfloat16
        ),
        "tp",
        scatter_dimension=0,
        tiled=True,
    )


def expert_half(
    expert_hidden_state,
    chosen_expert_index,
    chosen_expert_score,
    expert_norm_gain,
    routed_gate_weight,
    routed_up_weight,
    routed_down_weight,
    shared_gate_weight,
    shared_up_weight,
    shared_down_weight,
):
    tokens, top = chosen_expert_index.shape
    local_experts = routed_gate_weight.shape[0]
    devices = lax.axis_size("ep")
    experts = local_experts * devices
    capacity = min(tokens, 2 * tokens * top // experts)
    width_out = routed_down_weight.shape[2]
    features = expert_hidden_state.astype(jnp.float32)
    normed = (
        features
        * lax.rsqrt(jnp.mean(features * features, axis=1, keepdims=True) + EPSILON)
        * expert_norm_gain[None, :]
    ).astype(jnp.bfloat16)
    gates = ROUTED_SCALE * chosen_expert_score / jnp.sum(chosen_expert_score, axis=1, keepdims=True)
    flat_ids = chosen_expert_index.reshape(-1)
    onehot = (flat_ids[:, None] == jnp.arange(experts, dtype=jnp.int32)[None, :]).astype(jnp.int32)
    places = jnp.sum(onehot * (jnp.cumsum(onehot, axis=0) - 1), axis=1)
    slots = flat_ids * capacity + places
    owners = (
        jnp.full((experts * capacity,), tokens, jnp.int32)
        .at[slots]
        .set(jnp.arange(tokens * top, dtype=jnp.int32) // top)
    )
    padded = jnp.concatenate([normed, jnp.zeros((1, normed.shape[1]), jnp.bfloat16)], axis=0)
    outgoing = padded[owners].reshape(experts, capacity, normed.shape[1])
    piece = lax.all_to_all(outgoing, "ep", split_axis=0, concat_axis=0, tiled=True)
    grouped = piece.reshape(devices, local_experts, piece.shape[1], piece.shape[2])
    gate_part = jnp.einsum(
        "secd,edh->sech", grouped, routed_gate_weight, preferred_element_type=jnp.float32
    )
    up_part = jnp.einsum(
        "secd,edh->sech", grouped, routed_up_weight, preferred_element_type=jnp.float32
    )
    hidden = (jax.nn.silu(gate_part) * up_part).astype(jnp.bfloat16)
    hidden_rows = hidden.reshape(devices * local_experts, piece.shape[1], hidden.shape[3])
    flat_hidden = hidden_rows.reshape(experts * capacity, hidden_rows.shape[2])
    shared_hidden = (
        jax.nn.silu(jnp.dot(normed, shared_gate_weight, preferred_element_type=jnp.float32))
        * jnp.dot(normed, shared_up_weight, preferred_element_type=jnp.float32)
    ).astype(jnp.bfloat16)
    start_values = (
        jnp.zeros((experts * capacity, width_out), jnp.float32),
        jnp.zeros((tokens, width_out), jnp.float32),
    )
    routed_piece = lax.all_gather(flat_hidden, "tp", axis=1, tiled=True)
    shared_piece = lax.all_gather(shared_hidden, "tp", axis=1, tiled=True)
    count = routed_piece.shape[1]
    grouped = routed_piece.reshape(devices, local_experts, capacity, count)
    routed = jnp.einsum(
        "secn,enk->seck", grouped, routed_down_weight, preferred_element_type=jnp.float32
    )
    shared = jnp.dot(shared_piece, shared_down_weight, preferred_element_type=jnp.float32)
    routed_sum = routed.reshape(start_values[0].shape)
    answers = routed_sum.astype(jnp.bfloat16).reshape(experts, capacity, width_out)
    returned = lax.all_to_all(answers, "ep", split_axis=0, concat_axis=0, tiled=True)
    picked_rows = returned.reshape(experts * capacity, width_out)[slots].reshape(
        tokens, top, width_out
    )
    combined = shared + jnp.sum(gates[:, :, None] * picked_rows.astype(jnp.float32), axis=1)
    return combined.astype(jnp.bfloat16)


def dense_expert_half(
    expert_hidden_state,
    chosen_expert_index,
    chosen_expert_score,
    expert_norm_gain,
    routed_gate_weight,
    routed_up_weight,
    routed_down_weight,
    shared_gate_weight,
    shared_up_weight,
    shared_down_weight,
):
    tokens, top = chosen_expert_index.shape
    experts = lax.axis_size("ep")
    features = expert_hidden_state.astype(jnp.float32)
    width = features.shape[1]
    normed = (
        features
        * lax.rsqrt(jnp.mean(features * features, axis=1, keepdims=True) + EPSILON)
        * expert_norm_gain[None, :]
    ).astype(jnp.bfloat16)
    gates = ROUTED_SCALE * chosen_expert_score / jnp.sum(chosen_expert_score, axis=1, keepdims=True)
    chosen = chosen_expert_index[:, :, None] == jnp.arange(64, dtype=jnp.int32)[None, None, :]
    gate_table = jnp.sum(jnp.where(chosen, gates[:, :, None], 0.0), axis=1)
    high = gate_table.astype(jnp.bfloat16)
    low = (gate_table - high.astype(jnp.float32)).astype(jnp.bfloat16)
    sent = jnp.concatenate([normed, high, low], axis=1)
    everything = lax.all_gather(sent, "ep", axis=0, tiled=True)
    rows = everything[:, :width]
    mine = jnp.arange(64, dtype=jnp.int32) == lax.axis_index("ep")
    tail = everything[:, width:].astype(jnp.float32)
    own_gate = jnp.sum(jnp.where(mine[None, :], tail[:, :64] + tail[:, 64:], 0.0), axis=1)
    shared_hidden = (
        jax.nn.silu(jnp.dot(normed, shared_gate_weight, preferred_element_type=jnp.float32))
        * jnp.dot(normed, shared_up_weight, preferred_element_type=jnp.float32)
    ).astype(jnp.bfloat16)
    gate_part = jnp.dot(rows, routed_gate_weight[0], preferred_element_type=jnp.float32)
    up_part = jnp.dot(rows, routed_up_weight[0], preferred_element_type=jnp.float32)
    hidden = (jax.nn.silu(gate_part) * up_part * own_gate[:, None]).astype(jnp.bfloat16)
    shared_full = lax.all_gather(shared_hidden, "tp", axis=1, tiled=True)
    hidden_full = lax.all_gather(hidden, "tp", axis=1, tiled=True)
    shared = jnp.dot(shared_full, shared_down_weight, preferred_element_type=jnp.float32)
    routed = jnp.dot(hidden_full, routed_down_weight[0], preferred_element_type=jnp.float32).astype(
        jnp.bfloat16
    )
    total = lax.psum_scatter(routed, "ep", scatter_dimension=0, tiled=True)
    return (shared + total.astype(jnp.float32)).astype(jnp.bfloat16)


def per_device(
    recurrence_query_input,
    forget_gate_input,
    recurrence_value_input,
    output_gate_input,
    forget_lower_margin,
    position_decay_extra,
    head_norm_gain,
    recurrence_out_weight,
    expert_hidden_state,
    chosen_expert_index,
    chosen_expert_score,
    expert_norm_gain,
    routed_gate_weight,
    routed_up_weight,
    routed_down_weight,
    shared_gate_weight,
    shared_up_weight,
    shared_down_weight,
):
    recurrence_output = mixer_half(
        recurrence_query_input,
        forget_gate_input,
        recurrence_value_input,
        output_gate_input,
        forget_lower_margin,
        position_decay_extra,
        head_norm_gain,
        recurrence_out_weight,
    )
    tokens, top = chosen_expert_index.shape
    experts = routed_gate_weight.shape[0] * lax.axis_size("ep")
    every_row_fits = 2 * top >= experts and routed_gate_weight.shape[0] == 1 and (experts <= 64)
    half = dense_expert_half if every_row_fits else expert_half
    expert_out = half(
        expert_hidden_state,
        chosen_expert_index,
        chosen_expert_score,
        expert_norm_gain,
        routed_gate_weight,
        routed_up_weight,
        routed_down_weight,
        shared_gate_weight,
        shared_up_weight,
        shared_down_weight,
    )
    return (recurrence_output, expert_out)


def solution(mesh):
    in_specs = (
        P(("grp", "ep"), "tp"),
        P(("grp", "ep"), "tp"),
        P(("grp", "ep"), "tp"),
        P(("grp", "ep"), "tp"),
        P("tp"),
        P(("grp", "ep"), "tp"),
        P("tp"),
        P("tp", None),
        P(("grp", "ep"), None),
        P(("grp", "ep"), None),
        P(("grp", "ep"), None),
        P(),
        P("ep", None, "tp"),
        P("ep", None, "tp"),
        P("ep", None, "tp"),
        P(None, "tp"),
        P(None, "tp"),
        P(None, "tp"),
    )
    out_specs = (P(("grp", "ep", "tp"), None), P(("grp", "ep"), "tp"))
    return jax.shard_map(
        per_device, mesh=mesh, in_specs=in_specs, out_specs=out_specs, check_vma=False
    )
```

profile of v0, /device:TPU:0, one launch (start us, length us, event | category | flops | bytes accessed | tf_op | source)
XLA Modules:
  0.0 198.3 jit_solution(6184943672864648955)
XLA Ops:
  7.3 1.4 fusion.22
  16.9 1.9 fusion.38
  18.8 46.3 %all-gather.6.cloned.1.call-done = bf16[1024,2176]{1,0:T(8,128)(2,1)} async-done(((bf16[128,2176]{1,0:T(8,128)(2,1)}), bf16[1024,2176]{1,0:T(8,128)(2,1)}) %all-gather.6.cloned.1.call-update) | async-done | bytes 4456464 | tf_op jit(solution)/shard_map/all_gather | solution.py:219
  66.5 5.3 %fusion.3 = f32[1024,512]{1,0:T(8,128)S(1)} fusion(bf16[1024,2176]{1,0:T(8,128)(2,1)} %all-gather.6.cloned.1.call-done, bf16[1,2048,512]{2,1,0:T(8,128)(2,1)} %param.34), kind=kOutput, calls=%fused_computation.8 | convolution fusion | flops 2147483648 | bytes 8388608 | tf_op jit(solution)/shard_map/dot_general | solution.py:228
  71.9 3.6 %multiply_convert_fusion = bf16[1024,512]{1,0:T(8,128)(2,1)} fusion(f32[1024,512]{1,0:T(8,128)S(1)} %fusion.3, bf16[1,2048,512]{2,1,0:T(8,128)(2,1)S(1)} %copy-done.8, bf16[1024,2176]{1,0:T(8,128)(2,1)S(1)} %bitcast.139, f32[1024]{0:T(1024)S(1)} %fusion.37), kind=kOutput, calls=%fused_computation.15 | convolution fusion | flops 2151153664 | bytes 9441280 | tf_op jit(solution)/shard_map/dot_general | solution.py:229
  77.0 2.5 %bitcast_multiply_fusion.1 = (bf16[8,2,64,128]{3,0,1,2:T(8,128)(2,1)S(1)}, bf16[8,2,64,128]{3,0,1,2:T(8,128)(2,1)}, bf16[8,2,64,128]{3,0,1,2:T(8,128)(2,1)}, bf16[8,2,64,128]{3,0,1,2:T(8,128)(2,1)}) fusion(f32[8,2,64,128]{3,0,1,2:T(8,128)} %fusion.38, f32[8,2,128]{2,0,1:T(8,128)S(1)} %get-tuple-element.192, f32[8,2,128]{2,0,1:T(8,128)S(1)} %get-tuple-element.193, ...), kind=kLoop, calls=%fused_computation.54 | loop fusion | flops 1441792 | bytes 2637824 | tf_op jit(solution)/shard_map/mul | solution.py:82
  79.5 1.3 fusion.41
  80.8 4.5 %while.27 = (s32[]{:T(128)}, f32[8,128,128]{2,1,0:T(8,128)S(1)}, f32[2,8,128,128]{3,2,1,0:T(8,128)}, f32[2,8,128]{2,1,0:T(8,128)S(1)}, f32[2,8,128,128]{3,2,1,0:T(8,128)}, /*index=5*/s32[]{:T(128)}, s32[]{:T(128)}) while((s32[]{:T(128)}, f32[8,128,128]{2,1,0:T(8,128)S(1)}, f32[2,8,128,128]{3,2,1,0:T(8,128)}, ...), condition=%wide.region_2.3_spmd.clone, body=%wide.region_1.2_spmd.clone.sunk | while | flops 524291 | bytes 2633836 | solution.py:94
  81.7 1.4 bitcast_add_fusion.3
  83.9 1.4 bitcast_add_fusion.3
  86.2 12.8 %all-gather = bf16[64,128]{1,0:T(8,128)(2,1)S(1)} all-gather(bf16[8,128]{1,0:T(8,128)(2,1)S(1)} %exponential_convert_fusion), channel_id=2, replica_groups=mesh['grp'=2,'ep'=8,'tp'=2] {'ep'}, dimensions={0}, use_global_device_ids=true | all-gather | bytes 18432 | tf_op jit(solution)/shard_map/all_gather | solution.py:16
  100.5 7.1 %all-gather.8.cloned.1.call-done = bf16[1024,1024]{1,0:T(8,128)(2,1)} async-done(((bf16[1024,512]{1,0:T(8,128)(2,1)}), bf16[1024,1024]{1,0:T(8,128)(2,1)}) %all-gather.8.cloned.1.call-update) | async-done | bytes 2097168 | tf_op jit(solution)/shard_map/all_gather | solution.py:232
  107.6 5.2 %fusion.9 = bf16[1024,1024]{1,0:T(8,128)(2,1)} fusion(bf16[1024,1024]{1,0:T(8,128)(2,1)} %all-gather.8.cloned.1.call-done, bf16[1,1024,1024]{2,1,0:T(8,128)(2,1)S(1)} %copy-done), kind=kOutput, calls=%fused_computation.16 | convolution fusion | flops 2148532224 | bytes 6291456 | tf_op jit(solution)/shard_map/dot_general | solution.py:234
  113.7 2.2 %fusion.17 = f32[8,2,64,128]{3,2,1,0:T(8,128)} fusion(bf16[8,2,64,128]{3,0,1,2:T(8,128)(2,1)S(1)} %copy-done.4, bf16[8,2,64,128]{3,0,1,2:T(8,128)(2,1)} %get-tuple-element.189, bf16[8,2,64,128]{3,0,2,1:T(8,128)(2,1)} %bitcast_bitcast_fusion, pred[64,64]{1,0:T(8,128)(4,1)S(1)} %iota_compare_fusion.1), kind=kOutput, calls=%fused_computation.22 | convolution fusion | flops 33619968 | bytes 1314816 | tf_op jit(solution)/shard_map/hncs,hnse->hnce/dot_general | solution.py:79
  115.9 22.4 %all-gather.10.cloned.1.call-done = bf16[64,128,128]{2,1,0:T(8,128)(2,1)} async-done(((bf16[8,128,128]{2,1,0:T(8,128)(2,1)}), bf16[64,128,128]{2,1,0:T(8,128)(2,1)}) %all-gather.10.cloned.1.call-update) | async-done | bytes 2097168 | tf_op jit(solution)/shard_map/all_gather | solution.py:16
  138.3 10.8 %while.28 = (s32[]{:T(128)}, f32[8,128,128]{2,1,0:T(8,128)S(1)}, s32[]{:T(128)}, bf16[8,8,128]{2,1,0:T(8,128)(2,1)S(1)}, bf16[8,8,128,128]{3,2,1,0:T(8,128)(2,1)}, /*index=5*/s32[]{:T(128)}, s32[]{:T(128)}) while((s32[]{:T(128)}, f32[8,128,128]{2,1,0:T(8,128)S(1)}, s32[]{:T(128)}, bf16[8,8,128]{2,1,0:T(8,128)(2,1)S(1)}, ...), condition=%wide.region_6.7_spmd.clone, body=%wide.region_5.6_spmd.clone.sunk | while | flops 656388 | bytes 1321073 | solution.py:33
  138.3 1.3 fusion.73
  139.7 1.3 fusion.73
  141.1 1.3 fusion.73
  142.4 1.3 fusion.73
  143.8 1.3 fusion.73
  145.1 1.3 fusion.73
  146.5 1.3 fusion.73
  147.8 1.3 fusion.73
  149.2 2.7 %multiply_reduce_fusion = (f32[2,64,8]{1,0,2:T(2,128)S(1)}, f32[2,64,8,128]{3,1,0,2:T(8,128)}) fusion(f32[8,2,64,128]{3,2,1,0:T(8,128)} %fusion.17, bf16[8,2,64,128]{3,0,1,2:T(8,128)(2,1)S(1)} %copy-done.1, f32[2,8,128,128]{3,2,1,0:T(8,128)} %get-tuple-element.124, f32[8,128,128]{2,1,0:T(8,128)S(1)} %get-tuple-element.126, f32[2,8,128]{2,1,0:T(8,128)S(1)} %fusion.21), kind=kOutput, calls=%fused_computation.66 | convolution fusion | flops 34733056 | bytes 2895872 | tf_op jit(solution)/shard_map/hncd,nhde->hnce/dot_general | solution.py:100
  151.9 1.4 copy.67
  153.5 4.0 %convolution_convert_fusion = bf16[128,2048]{1,0:T(8,128)(2,1)} fusion(bf16[1024,2048]{1,0:T(8,128)(2,1)} %param.29, bf16[128,1024]{1,0:T(8,128)(2,1)} %param.25, f32[16,8,8,128]{3,2,1,0:T(8,128)S(1)} %bitcast.133, f32[16,8,8,128]{3,2,1,0:T(8,128)S(1)} %bitcast.134, f32[1024]{0:T(1024)S(1)} %copy-done.10), kind=kOutput, calls=%fused_computation.10 | convolution fusion | flops 538312704 | bytes 6033408 | tf_op jit(solution)/shard_map/dot_general | solution.py:110
  157.6 2.2 %fusion.60 = f32[128,512]{1,0:T(8,128)S(1)} fusion(bf16[128,2048]{1,0:T(8,128)(2,1)S(1)} %fusion.24, bf16[2048,512]{1,0:T(8,128)(2,1)} %param.37), kind=kOutput, calls=%fused_computation.94 | convolution fusion | flops 268435456 | bytes 2883584 | tf_op jit(solution)/shard_map/dot_general | solution.py:225
  160.3 6.3 %all_gather.22 = bf16[128,1024]{1,0:T(8,128)(2,1)S(1)} all-gather(bf16[128,512]{1,0:T(8,128)(2,1)S(1)} %fusion.19), channel_id=1, replica_groups=mesh['grp'=2,'ep'=8,'tp'=2] {'tp'}, dimensions={1}, use_global_device_ids=true | all-gather | bytes 393216 | tf_op jit(solution)/shard_map/all_gather | solution.py:231
  166.6 9.4 %reduce-scatter.5.cloned.1.call-done = bf16[128,1024]{1,0:T(8,128)(2,1)} async-done(((bf16[1024,1024]{1,0:T(8,128)(2,1)}), bf16[128,1024]{1,0:T(8,128)(2,1)}) %reduce-scatter.5.cloned.1.call-update) | async-done | bytes 262160 | tf_op jit(solution)/shard_map/reduce_scatter | solution.py:237
  176.0 2.7 %fusion.18 = bf16[128,1024]{1,0:T(8,128)(2,1)} fusion(bf16[128,1024]{1,0:T(8,128)(2,1)S(1)} %all_gather.22, bf16[1024,1024]{1,0:T(8,128)(2,1)} %param.39, bf16[128,1024]{1,0:T(8,128)(2,1)} %reduce-scatter.5.cloned.1.call-done), kind=kOutput, calls=%fused_computation.24 | convolution fusion | flops 268828672 | bytes 2883584 | tf_op jit(solution)/shard_map/dot_general | solution.py:233
  178.7 13.0 %reduce-scatter.3.cloned.1.call-done = bf16[64,2048]{1,0:T(8,128)(2,1)} async-done(((bf16[128,2048]{1,0:T(8,128)(2,1)}), bf16[64,2048]{1,0:T(8,128)(2,1)}) %reduce-scatter.3.cloned.1.call-update) | async-done | bytes 262160 | tf_op jit(solution)/shard_map/reduce_scatter | solution.py:109
  (83 shorter events, 16.9 us)
Async XLA Ops:
  7.2 100.4 %copy-start = (bf16[1,1024,1024]{2,1,0:T(8,128)(2,1)S(1)}, bf16[1,1024,1024]{2,1,0:T(8,128)(2,1)}, u32[]{:S(2)}) copy-start(bf16[1,1024,1024]{2,1,0:T(8,128)(2,1)} %param.36) | copy-start | bytes 6291460
  7.2 6.1 %copy-start.7 = (f32[128,8]{0,1:T(8,128)S(1)}, f32[128,8]{0,1:T(8,128)}, u32[]{:S(2)}) copy-start(f32[128,8]{0,1:T(8,128)} %param.27) | copy-start | bytes 12292
  7.2 6.4 %copy-start.2 = (bf16[128,1024]{1,0:T(8,128)(2,1)S(1)}, bf16[128,1024]{1,0:T(8,128)(2,1)}, u32[]{:S(2)}) copy-start(bf16[128,1024]{1,0:T(8,128)(2,1)} %param.23) | copy-start | bytes 786436
  7.2 6.4 %copy-start.6 = (f32[1024]{0:T(1024)S(1)}, f32[1024]{0:T(1024)}, u32[]{:S(2)}) copy-start(f32[1024]{0:T(1024)} %param.26) | copy-start | bytes 12292
  7.2 57.9 %all-gather.6.cloned.1.call-start = ((), (), s32[]{:S(2)}) async-start(), calls=%async_computation.3 | async-start | bytes 5013504 | tf_op jit(solution)/shard_map/all_gather | solution.py:219
  13.2 94.3 %all-gather.8.cloned.1.call-start = ((), (), s32[]{:S(2)}) async-start(), calls=%async_computation.4 | async-start | bytes 3145728 | tf_op jit(solution)/shard_map/all_gather | solution.py:232
  13.4 1.5 copy-start.3
  14.0 2.9 %copy-start.5 = (bf16[128,1024]{1,0:T(8,128)(2,1)S(1)}, bf16[128,1024]{1,0:T(8,128)(2,1)}, u32[]{:S(2)}) copy-start(bf16[128,1024]{1,0:T(8,128)(2,1)} %param.24) | copy-start | bytes 786436
  66.1 5.8 %slice-start = ((s8[4456448]{0:T(1024)(128)(4,1)}), s8[4194304]{0:T(1024)(128)(4,1)S(1)}, s32[]{:S(2)}) async-start(s8[4456448]{0:T(1024)(128)(4,1)} %bitcast.138), calls=%async_computation.7 | async-start | bytes 8388608
  66.5 5.4 %slice-start.1 = ((s8[4456448]{0:T(1024)(128)(4,1)}), s8[262144]{0:T(1024)(128)(4,1)S(1)}, s32[]{:S(2)}) async-start(s8[4456448]{0:T(1024)(128)(4,1)} %bitcast.138), calls=%async_computation.8 | async-start | bytes 524288
  66.5 5.4 %copy-start.8 = (bf16[1,2048,512]{2,1,0:T(8,128)(2,1)S(1)}, bf16[1,2048,512]{2,1,0:T(8,128)(2,1)}, u32[]{:S(2)}) copy-start(bf16[1,2048,512]{2,1,0:T(8,128)(2,1)} %param.35) | copy-start | bytes 6291460
  75.5 62.8 %all-gather.10.cloned.1.call-start = ((), (), s32[]{:S(2)}) async-start(), calls=%async_computation.6 | async-start | bytes 2359296 | tf_op jit(solution)/shard_map/all_gather | solution.py:16
  86.1 89.9 %reduce-scatter.5.cloned.1.call-start = ((), (), s32[]{:S(2)}) async-start(), calls=%async_computation.5 | async-start | bytes 2359296 | tf_op jit(solution)/shard_map/reduce_scatter | solution.py:237
  112.8 0.9 copy-start.4
  112.8 79.0 %reduce-scatter.3.cloned.1.call-start = ((), (), s32[]{:S(2)}) async-start(), calls=%async_computation.2 | async-start | bytes 786432 | tf_op jit(solution)/shard_map/reduce_scatter | solution.py:109
  138.3 10.8 %copy-start.1 = (bf16[8,2,64,128]{3,0,1,2:T(8,128)(2,1)S(1)}, bf16[8,2,64,128]{3,0,1,2:T(8,128)(2,1)}, u32[]{:S(2)}) copy-start(bf16[8,2,64,128]{3,0,1,2:T(8,128)(2,1)} %get-tuple-element.190) | copy-start | bytes 786436
  149.1 4.3 %copy-start.10 = (f32[1024]{0:T(1024)S(1)}, f32[1024]{0:T(1024)}, u32[]{:S(2)}) copy-start(f32[1024]{0:T(1024)} %param.28) | copy-start | bytes 12292
  157.5 2.3 %copy-start.9 = (bf16[2048,512]{1,0:T(8,128)(2,1)S(1)}, bf16[2048,512]{1,0:T(8,128)(2,1)}, u32[]{:S(2)}) copy-start(bf16[2048,512]{1,0:T(8,128)(2,1)} %param.38) | copy-start | bytes 6291460
Sparse Core Ops, SparseCore 0:
  13.4 51.7 all-gather.5
  75.6 31.8 all-gather.7
  109.2 29.1 all-gather.9
  140.5 35.4 reduce-scatter.4
  178.7 13.0 reduce-scatter.2
where the time goes:
time: 199 us; the launch traced here: 198 us
  waiting for transfers between devices  98.3 us (49%)
  matrix products  29.8 us (15%)
  other arithmetic  28.2 us (14%)
  blocking collectives  19.1 us (10%)
  between operations  14.1 us (7%)
  local copies, waits for them, and re-layouts  8.28 us (4%)
    all_gather x1, waiting for transfers between devices, dense_expert_half(): everything = lax.all_gather(sent, 'ep', axis=0, tiled=True)  46.3 us
    all_gather x1, waiting for transfers between devices, carried_in(): lax.all_gather(part.astype(kind), axis)  22.4 us
    reduce_scatter x1, waiting for transfers between devices, mixer_half(): lax.psum_scatter(jnp.dot(gated_rows, recurrence_out_weight, preferred_ele...  13 us
    all_gather x1, blocking collectives, carried_in(): lax.all_gather(part.astype(kind), axis)  12.8 us
    select_n x8, other arithmetic, turn(): return jax.tree.map(lambda a, b: jnp.where(reached, a, b), new, before)  10.4 us
    reduce_scatter x1, waiting for transfers between devices, dense_expert_half(): total = lax.psum_scatter(routed, 'ep', scatter_dimension=0, tiled=True)  9.4 us
    all_gather x1, waiting for transfers between devices, dense_expert_half(): hidden_full = lax.all_gather(hidden, 'tp', axis=1, tiled=True)  7.09 us
    all_gather x1, blocking collectives, dense_expert_half(): shared_full = lax.all_gather(shared_hidden, 'tp', axis=1, tiled=True)  6.33 us
  transfers between devices with their start and end apart: 5, of which 5 were waited for; matrix products, arithmetic and copies ran while one was open for 25% of the time, Pallas kernels for 0%

commit v1 on v0

--- a/solution.py
+++ b/solution.py
@@ -216,7 +216,12 @@
     high = gate_table.astype(jnp.bfloat16)
     low = (gate_table - high.astype(jnp.float32)).astype(jnp.bfloat16)
     sent = jnp.concatenate([normed, high, low], axis=1)
-    everything = lax.all_gather(sent, "ep", axis=0, tiled=True)
+    ring = [sent]
+    for hop in range(7):
+        ring.append(lax.ppermute(ring[-1], "ep", [(dev, (dev + 1) % 8) for dev in range(8)]))
+    everything = jnp.roll(
+        jnp.concatenate(ring[::-1], axis=0), (lax.axis_index("ep") + 1) * ring[0].shape[0], axis=0
+    )
     rows = everything[:, :width]
     mine = jnp.arange(64, dtype=jnp.int32) == lax.axis_index("ep")
     tail = everything[:, width:].astype(jnp.float32)

time: 199 us -> 231 us (1.16)
  waiting for transfers between devices: 98.3 us -> 125 us
  local copies, waits for them, and re-layouts: 8.28 us -> 16.3 us
    ppermute x0 -> x7, waiting for transfers between devices: none -> 69.1 us  [dense_expert_half(): lax.ppermute(ring[-1], 'ep', [(dev, (dev + 1) % 8) for dev in range(8)])]
    all_gather x1 -> x0, waiting for transfers between devices: 46.3 us -> none  [dense_expert_half(): everything = lax.all_gather(sent, 'ep', axis=0, tiled=True)]
    unnamed x31 -> x60, local copies, waits for them, and re-layouts: 3.83 us -> 14.2 us
    dot_general x1, matrix products: 5.35 us -> 2.32 us  [dense_expert_half(): jnp.dot(rows, routed_gate_weight[0], preferred_element_type=jnp.float32)]
  transfers between devices with their start and end apart: 5 -> 11, of which waited for: 5 -> 11; matrix products, arithmetic and copies ran while one was open for 25% -> 21% of each run, Pallas kernels for 0% -> 0%
where the time goes in v1:
time: 231 us; the launch traced here: 230 us
  waiting for transfers between devices  125 us (54%)
  matrix products  27.5 us (12%)
  other arithmetic  26.7 us (12%)
  blocking collectives  19.1 us (8%)
  local copies, waits for them, and re-layouts  16.3 us (7%)
  between operations  14.3 us (6%)
    ppermute x7, waiting for transfers between devices, dense_expert_half(): lax.ppermute(ring[-1], 'ep', [(dev, (dev + 1) % 8) for dev in range(8)])  69.1 us
    all_gather x1, waiting for transfers between devices, carried_in(): lax.all_gather(part.astype(kind), axis)  23.1 us
    unnamed x60, local copies, waits for them, and re-layouts  14.2 us
    reduce_scatter x1, waiting for transfers between devices, mixer_half(): lax.psum_scatter(jnp.dot(gated_rows, recurrence_out_weight, preferred_ele...  13.3 us
    all_gather x1, blocking collectives, carried_in(): lax.all_gather(part.astype(kind), axis)  12.8 us
    select_n x8, other arithmetic, turn(): return jax.tree.map(lambda a, b: jnp.where(reached, a, b), new, before)  10.4 us
    reduce_scatter x1, waiting for transfers between devices, dense_expert_half(): total = lax.psum_scatter(routed, 'ep', scatter_dimension=0, tiled=True)  9.76 us
    all_gather x1, waiting for transfers between devices, dense_expert_half(): hidden_full = lax.all_gather(hidden, 'tp', axis=1, tiled=True)  9.3 us
  transfers between devices with their start and end apart: 11, of which 11 were waited for; matrix products, arithmetic and copies ran while one was open for 21% of the time, Pallas kernels for 0%

profile of v1, /device:TPU:0, one launch (start us, length us, event | category | flops | bytes accessed | tf_op | source)
XLA Modules:
  0.0 229.7 jit_solution(13747886686071996286)
XLA Ops:
  7.2 1.4 fusion.18
  13.1 11.2 %collective-permute-done = bf16[128,2176]{1,0:T(8,128)(2,1)S(1)} collective-permute-done((bf16[128,2176]{1,0:T(8,128)(2,1)S(1)}, bf16[128,2176]{1,0:T(8,128)(2,1)S(1)}, u32[]{:S(2)}, u32[]{:S(2)}) %collective-permute-start) | collective-permute-done | bytes 557088 | tf_op jit(solution)/shard_map/ppermute | solution.py:221
  25.1 10.8 %collective-permute-done.1 = bf16[128,2176]{1,0:T(8,128)(2,1)S(1)} collective-permute-done((bf16[128,2176]{1,0:T(8,128)(2,1)S(1)}, bf16[128,2176]{1,0:T(8,128)(2,1)S(1)}, u32[]{:S(2)}, u32[]{:S(2)}) %collective-permute-start.1) | collective-permute-done | bytes 557088 | tf_op jit(solution)/shard_map/ppermute | solution.py:221
  36.7 10.8 %collective-permute-done.2 = bf16[128,2176]{1,0:T(8,128)(2,1)S(1)} collective-permute-done((bf16[128,2176]{1,0:T(8,128)(2,1)S(1)}, bf16[128,2176]{1,0:T(8,128)(2,1)S(1)}, u32[]{:S(2)}, u32[]{:S(2)}) %collective-permute-start.2) | collective-permute-done | bytes 557088 | tf_op jit(solution)/shard_map/ppermute | solution.py:221
  48.3 10.8 %collective-permute-done.3 = bf16[128,2176]{1,0:T(8,128)(2,1)S(1)} collective-permute-done((bf16[128,2176]{1,0:T(8,128)(2,1)S(1)}, bf16[128,2176]{1,0:T(8,128)(2,1)S(1)}, u32[]{:S(2)}, u32[]{:S(2)}) %collective-permute-start.3) | collective-permute-done | bytes 557088 | tf_op jit(solution)/shard_map/ppermute | solution.py:221
  59.8 10.9 %collective-permute-done.4 = bf16[128,2176]{1,0:T(8,128)(2,1)} collective-permute-done((bf16[128,2176]{1,0:T(8,128)(2,1)S(1)}, bf16[128,2176]{1,0:T(8,128)(2,1)}, u32[]{:S(2)}, u32[]{:S(2)}) %collective-permute-start.4) | collective-permute-done | bytes 557088 | tf_op jit(solution)/shard_map/ppermute | solution.py:221
  74.8 7.0 %collective-permute-done.5 = bf16[128,2176]{1,0:T(8,128)(2,1)} collective-permute-done((bf16[128,2176]{1,0:T(8,128)(2,1)}, bf16[128,2176]{1,0:T(8,128)(2,1)}, u32[]{:S(2)}, u32[]{:S(2)}) %collective-permute-start.5) | collective-permute-done | bytes 557088 | tf_op jit(solution)/shard_map/ppermute | solution.py:221
  83.0 2.1 fusion.34
  85.0 7.8 %collective-permute-done.6 = bf16[128,2176]{1,0:T(8,128)(2,1)} collective-permute-done((bf16[128,2176]{1,0:T(8,128)(2,1)}, bf16[128,2176]{1,0:T(8,128)(2,1)}, u32[]{:S(2)}, u32[]{:S(2)}) %collective-permute-start.6) | collective-permute-done | bytes 557088 | tf_op jit(solution)/shard_map/ppermute | solution.py:221
  100.4 2.3 %fusion.3 = f32[1024,512]{1,0:T(8,128)S(1)} fusion(bf16[2048,2176]{1,0:T(8,128)(2,1)S(1)} %constant_dynamic-update-slice_fusion, s32[]{:T(128)S(6)} %select_n.52, bf16[1,2048,512]{2,1,0:T(8,128)(2,1)S(1)} %copy-done.17), kind=kOutput, calls=%fused_computation.8 | convolution fusion | flops 2147483648 | bytes 8388612 | tf_op jit(solution)/shard_map/dot_general | solution.py:233
  103.1 3.6 %multiply_convert_fusion = bf16[1024,512]{1,0:T(8,128)(2,1)} fusion(f32[1024,512]{1,0:T(8,128)S(1)} %fusion.3, f32[1024]{0:T(1024)S(1)} %fusion.33, bf16[1,2048,512]{2,1,0:T(8,128)(2,1)S(1)} %copy-done.18, bf16[2048,2176]{1,0:T(8,128)(2,1)S(1)} %constant_dynamic-update-slice_fusion, s32[]{:T(128)S(6)} %select_n.52), kind=kOutput, calls=%fused_computation.15 | convolution fusion | flops 2151153664 | bytes 9441284 | tf_op jit(solution)/shard_map/dot_general | solution.py:234
  106.8 2.3 %bitcast_multiply_fusion.1 = (bf16[8,2,64,128]{3,0,1,2:T(8,128)(2,1)S(1)}, bf16[8,2,64,128]{3,0,1,2:T(8,128)(2,1)}, bf16[8,2,64,128]{3,0,1,2:T(8,128)(2,1)}, bf16[8,2,64,128]{3,0,1,2:T(8,128)(2,1)}) fusion(f32[8,2,64,128]{3,0,1,2:T(8,128)S(1)} %copy-done.3, f32[8,2,128]{2,0,1:T(8,128)S(1)} %get-tuple-element.192, f32[8,2,128]{2,0,1:T(8,128)S(1)} %get-tuple-element.193, ...), kind=kLoop, calls=%fused_computation.54 | loop fusion | flops 1441792 | bytes 2637824 | tf_op jit(solution)/shard_map/mul | solution.py:82
  109.2 1.4 fusion.37
  110.5 4.4 %while.27 = (s32[]{:T(128)}, f32[8,128,128]{2,1,0:T(8,128)S(1)}, f32[2,8,128,128]{3,2,1,0:T(8,128)}, f32[2,8,128]{2,1,0:T(8,128)S(1)}, f32[2,8,128,128]{3,2,1,0:T(8,128)}, /*index=5*/s32[]{:T(128)}, s32[]{:T(128)}) while((s32[]{:T(128)}, f32[8,128,128]{2,1,0:T(8,128)S(1)}, f32[2,8,128,128]{3,2,1,0:T(8,128)}, ...), condition=%wide.region_2.3_spmd.clone, body=%wide.region_1.2_spmd.clone.sunk | while | flops 524291 | bytes 2634336 | solution.py:94
  111.4 1.4 bitcast_add_fusion.3
  113.6 1.3 bitcast_add_fusion.3
  115.8 12.8 %all-gather = bf16[64,128]{1,0:T(8,128)(2,1)S(1)} all-gather(bf16[8,128]{1,0:T(8,128)(2,1)S(1)} %exponential_convert_fusion), channel_id=2, replica_groups=mesh['grp'=2,'ep'=8,'tp'=2] {'ep'}, dimensions={0}, use_global_device_ids=true | all-gather | bytes 18432 | tf_op jit(solution)/shard_map/all_gather | solution.py:16
  129.4 9.3 %all-gather.5.cloned.1.call-done = bf16[1024,1024]{1,0:T(8,128)(2,1)} async-done(((bf16[1024,512]{1,0:T(8,128)(2,1)}), bf16[1024,1024]{1,0:T(8,128)(2,1)}) %all-gather.5.cloned.1.call-update) | async-done | bytes 2097168 | tf_op jit(solution)/shard_map/all_gather | solution.py:237
  138.7 5.3 %fusion.9 = bf16[1024,1024]{1,0:T(8,128)(2,1)} fusion(bf16[1024,1024]{1,0:T(8,128)(2,1)} %all-gather.5.cloned.1.call-done, bf16[1,1024,1024]{2,1,0:T(8,128)(2,1)S(1)} %copy-done), kind=kOutput, calls=%fused_computation.16 | convolution fusion | flops 2148532224 | bytes 6291456 | tf_op jit(solution)/shard_map/dot_general | solution.py:239
  144.2 2.1 fusion.13
  146.4 23.1 %all-gather.7.cloned.1.call-done = bf16[64,128,128]{2,1,0:T(8,128)(2,1)} async-done(((bf16[8,128,128]{2,1,0:T(8,128)(2,1)}), bf16[64,128,128]{2,1,0:T(8,128)(2,1)}) %all-gather.7.cloned.1.call-update) | async-done | bytes 2097168 | tf_op jit(solution)/shard_map/all_gather | solution.py:16
  169.5 10.7 %while.28 = (s32[]{:T(128)}, f32[8,128,128]{2,1,0:T(8,128)S(1)}, s32[]{:T(128)}, bf16[8,8,128]{2,1,0:T(8,128)(2,1)S(1)}, bf16[8,8,128,128]{3,2,1,0:T(8,128)(2,1)}, /*index=5*/s32[]{:T(128)}, s32[]{:T(128)}) while((s32[]{:T(128)}, f32[8,128,128]{2,1,0:T(8,128)S(1)}, s32[]{:T(128)}, bf16[8,8,128]{2,1,0:T(8,128)(2,1)S(1)}, ...), condition=%wide.region_6.7_spmd.clone, body=%wide.region_5.6_spmd.clone.sunk | while | flops 656388 | bytes 1321065 | solution.py:33
  169.5 1.3 fusion.75
  176.2 1.3 fusion.75
  180.2 2.0 multiply_reduce_fusion
  182.8 4.0 %convolution_convert_fusion = bf16[128,2048]{1,0:T(8,128)(2,1)} fusion(bf16[1024,2048]{1,0:T(8,128)(2,1)} %param.29, bf16[128,1024]{1,0:T(8,128)(2,1)} %param.25, f32[16,8,8,128]{3,2,1,0:T(8,128)S(1)} %bitcast.133, f32[16,8,8,128]{3,2,1,0:T(8,128)S(1)} %bitcast.134, f32[1024]{0:T(1024)S(1)} %copy-done.19), kind=kOutput, calls=%fused_computation.10 | convolution fusion | flops 538312704 | bytes 6033408 | tf_op jit(solution)/shard_map/dot_general | solution.py:110
  186.9 2.1 fusion.62
  188.9 2.1 fusion.15
  191.0 6.3 %all_gather.19 = bf16[128,1024]{1,0:T(8,128)(2,1)S(1)} all-gather(bf16[128,512]{1,0:T(8,128)(2,1)S(1)} %fusion.15), channel_id=1, replica_groups=mesh['grp'=2,'ep'=8,'tp'=2] {'tp'}, dimensions={1}, use_global_device_ids=true | all-gather | bytes 393216 | tf_op jit(solution)/shard_map/all_gather | solution.py:236
  197.3 9.8 %reduce-scatter.5.cloned.1.call-done = bf16[128,1024]{1,0:T(8,128)(2,1)} async-done(((bf16[1024,1024]{1,0:T(8,128)(2,1)}), bf16[128,1024]{1,0:T(8,128)(2,1)}) %reduce-scatter.5.cloned.1.call-update) | async-done | bytes 262160 | tf_op jit(solution)/shard_map/reduce_scatter | solution.py:242
  207.1 2.7 %fusion.14 = bf16[128,1024]{1,0:T(8,128)(2,1)} fusion(bf16[128,1024]{1,0:T(8,128)(2,1)S(1)} %all_gather.19, bf16[1024,1024]{1,0:T(8,128)(2,1)} %param.39, bf16[128,1024]{1,0:T(8,128)(2,1)} %reduce-scatter.5.cloned.1.call-done), kind=kOutput, calls=%fused_computation.24 | convolution fusion | flops 268828672 | bytes 2883584 | tf_op jit(solution)/shard_map/dot_general | solution.py:238
  209.8 13.3 %reduce-scatter.3.cloned.1.call-done = bf16[64,2048]{1,0:T(8,128)(2,1)} async-done(((bf16[128,2048]{1,0:T(8,128)(2,1)}), bf16[64,2048]{1,0:T(8,128)(2,1)}) %reduce-scatter.3.cloned.1.call-update) | async-done | bytes 262160 | tf_op jit(solution)/shard_map/reduce_scatter | solution.py:109
  (123 shorter events, 32.8 us)
Async XLA Ops:
  7.2 131.5 %copy-start = (bf16[1,1024,1024]{2,1,0:T(8,128)(2,1)S(1)}, bf16[1,1024,1024]{2,1,0:T(8,128)(2,1)}, u32[]{:S(2)}) copy-start(bf16[1,1024,1024]{2,1,0:T(8,128)(2,1)} %param.36) | copy-start | bytes 6291460
  7.2 74.6 %copy-start.13 = (bf16[128,1024]{1,0:T(8,128)(2,1)S(1)}, bf16[128,1024]{1,0:T(8,128)(2,1)}, u32[]{:S(2)}) copy-start(bf16[128,1024]{1,0:T(8,128)(2,1)} %param.22) | copy-start | bytes 786436
  7.2 131.5 %all-gather.5.cloned.1.call-start = ((), (), s32[]{:S(2)}) async-start(), calls=%async_computation.3 | async-start | bytes 3145728 | tf_op jit(solution)/shard_map/all_gather | solution.py:237
  12.2 58.5 %copy-start.1 = (bf16[128,2048]{1,0:T(8,128)(2,1)}, bf16[128,2048]{1,0:T(8,128)(2,1)S(1)}, u32[]{:S(2)}) copy-start(bf16[128,2048]{1,0:T(8,128)(2,1)S(1)} %fusion.20) | copy-start | bytes 1572868
  12.5 11.8 %collective-permute-start = (bf16[128,2176]{1,0:T(8,128)(2,1)S(1)}, bf16[128,2176]{1,0:T(8,128)(2,1)S(1)}, u32[]{:S(2)}, u32[]{:S(2)}) collective-permute-start(bf16[128,2176]{1,0:T(8,128)(2,1)S(1)} %concatenate.9), channel_id=1, source_target_pairs={{0,2},{2,4},{4,6},{6,8},{8,10},{10,12},{12,14},{14,0},{1,3},{3,5},... | collective-permute-start | bytes 1671176 | tf_op jit(solution)/shard_map/ppermute | solution.py:221
  24.3 0.8 copy-start.4
  25.1 10.8 %collective-permute-start.1 = (bf16[128,2176]{1,0:T(8,128)(2,1)S(1)}, bf16[128,2176]{1,0:T(8,128)(2,1)S(1)}, u32[]{:S(2)}, u32[]{:S(2)}) collective-permute-start(bf16[128,2176]{1,0:T(8,128)(2,1)S(1)} %collective-permute-done), channel_id=1, source_target_pairs={{0,2},{2,4},{4,6},{6,8},{8,10},{10,12},{12,14},{14,0},{1,3},{3,5},... | collective-permute-start | bytes 1671176 | tf_op jit(solution)/shard_map/ppermute | solution.py:221
  35.9 0.8 copy-start.6
  36.7 10.8 %collective-permute-start.2 = (bf16[128,2176]{1,0:T(8,128)(2,1)S(1)}, bf16[128,2176]{1,0:T(8,128)(2,1)S(1)}, u32[]{:S(2)}, u32[]{:S(2)}) collective-permute-start(bf16[128,2176]{1,0:T(8,128)(2,1)S(1)} %collective-permute-done.1), channel_id=1, source_target_pairs={{0,2},{2,4},{4,6},{6,8},{8,10},{10,12},{12,14},{14,0},{1,3},{3,5},... | collective-permute-start | bytes 1671176 | tf_op jit(solution)/shard_map/ppermute | solution.py:221
  47.5 0.8 copy-start.8
  48.3 10.8 %collective-permute-start.3 = (bf16[128,2176]{1,0:T(8,128)(2,1)S(1)}, bf16[128,2176]{1,0:T(8,128)(2,1)S(1)}, u32[]{:S(2)}, u32[]{:S(2)}) collective-permute-start(bf16[128,2176]{1,0:T(8,128)(2,1)S(1)} %collective-permute-done.2), channel_id=1, source_target_pairs={{0,2},{2,4},{4,6},{6,8},{8,10},{10,12},{12,14},{14,0},{1,3},{3,5},... | collective-permute-start | bytes 1671176 | tf_op jit(solution)/shard_map/ppermute | solution.py:221
  59.0 0.8 copy-start.10
  59.8 10.9 %collective-permute-start.4 = (bf16[128,2176]{1,0:T(8,128)(2,1)S(1)}, bf16[128,2176]{1,0:T(8,128)(2,1)}, u32[]{:S(2)}, u32[]{:S(2)}) collective-permute-start(bf16[128,2176]{1,0:T(8,128)(2,1)S(1)} %collective-permute-done.3), channel_id=1, source_target_pairs={{0,2},{2,4},{4,6},{6,8},{8,10},{10,12},{12,14},{14,0},{1,3},{3,5},... | collective-permute-start | bytes 1671176 | tf_op jit(solution)/shard_map/ppermute | solution.py:221
  70.7 11.1 %collective-permute-start.5 = (bf16[128,2176]{1,0:T(8,128)(2,1)}, bf16[128,2176]{1,0:T(8,128)(2,1)}, u32[]{:S(2)}, u32[]{:S(2)}) collective-permute-start(bf16[128,2176]{1,0:T(8,128)(2,1)} %collective-permute-done.4), channel_id=1, source_target_pairs={{0,2},{2,4},{4,6},{6,8},{8,10},{10,12},{12,14},{14,0},{1,3},{3,5},... | collective-permute-start | bytes 1671176 | tf_op jit(solution)/shard_map/ppermute | solution.py:221
  71.5 11.3 %copy-start.16 = (bf16[128,1024]{1,0:T(8,128)(2,1)S(1)}, bf16[128,1024]{1,0:T(8,128)(2,1)}, u32[]{:S(2)}) copy-start(bf16[128,1024]{1,0:T(8,128)(2,1)} %param.24) | copy-start | bytes 786436
  81.8 11.1 %collective-permute-start.6 = (bf16[128,2176]{1,0:T(8,128)(2,1)}, bf16[128,2176]{1,0:T(8,128)(2,1)}, u32[]{:S(2)}, u32[]{:S(2)}) collective-permute-start(bf16[128,2176]{1,0:T(8,128)(2,1)} %collective-permute-done.5), channel_id=1, source_target_pairs={{0,2},{2,4},{4,6},{6,8},{8,10},{10,12},{12,14},{14,0},{1,3},{3,5},... | collective-permute-start | bytes 1671176 | tf_op jit(solution)/shard_map/ppermute | solution.py:221
  82.9 13.3 %copy-start.11 = (bf16[128,2176]{1,0:T(8,128)(2,1)S(1)}, bf16[128,2176]{1,0:T(8,128)(2,1)}, u32[]{:S(2)}) copy-start(bf16[128,2176]{1,0:T(8,128)(2,1)} %copy-done.10) | copy-start | bytes 1671172
  82.9 13.3 %copy-start.9 = (bf16[128,2176]{1,0:T(8,128)(2,1)S(1)}, bf16[128,2176]{1,0:T(8,128)(2,1)}, u32[]{:S(2)}) copy-start(bf16[128,2176]{1,0:T(8,128)(2,1)} %copy-done.8) | copy-start | bytes 1671172
  82.9 13.4 %copy-start.7 = (bf16[128,2176]{1,0:T(8,128)(2,1)S(1)}, bf16[128,2176]{1,0:T(8,128)(2,1)}, u32[]{:S(2)}) copy-start(bf16[128,2176]{1,0:T(8,128)(2,1)} %copy-done.6) | copy-start | bytes 1671172
  82.9 13.5 %copy-start.5 = (bf16[128,2176]{1,0:T(8,128)(2,1)S(1)}, bf16[128,2176]{1,0:T(8,128)(2,1)}, u32[]{:S(2)}) copy-start(bf16[128,2176]{1,0:T(8,128)(2,1)} %copy-done.4) | copy-start | bytes 1671172
  96.5 3.8 %copy-start.17 = (bf16[1,2048,512]{2,1,0:T(8,128)(2,1)S(1)}, bf16[1,2048,512]{2,1,0:T(8,128)(2,1)}, u32[]{:S(2)}) copy-start(bf16[1,2048,512]{2,1,0:T(8,128)(2,1)} %param.34) | copy-start | bytes 6291460
  100.4 2.8 %copy-start.18 = (bf16[1,2048,512]{2,1,0:T(8,128)(2,1)S(1)}, bf16[1,2048,512]{2,1,0:T(8,128)(2,1)}, u32[]{:S(2)}) copy-start(bf16[1,2048,512]{2,1,0:T(8,128)(2,1)} %param.35) | copy-start | bytes 6291460
  103.1 3.6 %copy-start.3 = (f32[8,2,64,128]{3,0,1,2:T(8,128)S(1)}, f32[8,2,64,128]{3,0,1,2:T(8,128)}, u32[]{:S(2)}) copy-start(f32[8,2,64,128]{3,0,1,2:T(8,128)} %fusion.34) | copy-start | bytes 1572868
  106.7 62.7 %all-gather.7.cloned.1.call-start = ((), (), s32[]{:S(2)}) async-start(), calls=%async_computation.5 | async-start | bytes 2359296 | tf_op jit(solution)/shard_map/all_gather | solution.py:16
  115.8 91.3 %reduce-scatter.5.cloned.1.call-start = ((), (), s32[]{:S(2)}) async-start(), calls=%async_computation.4 | async-start | bytes 2359296 | tf_op jit(solution)/shard_map/reduce_scatter | solution.py:242
  129.4 14.8 %copy-start.14 = (bf16[8,2,64,128]{3,0,1,2:T(8,128)(2,1)S(1)}, bf16[8,2,64,128]{3,0,1,2:T(8,128)(2,1)}, u32[]{:S(2)}) copy-start(bf16[8,2,64,128]{3,0,1,2:T(8,128)(2,1)} %get-tuple-element.188) | copy-start | bytes 786436
  129.4 14.8 %copy-start.15 = (bf16[8,2,64,128]{3,0,1,2:T(8,128)(2,1)S(1)}, bf16[8,2,64,128]{3,0,1,2:T(8,128)(2,1)}, u32[]{:S(2)}) copy-start(bf16[8,2,64,128]{3,0,1,2:T(8,128)(2,1)} %get-tuple-element.189) | copy-start | bytes 786436
  144.0 36.2 %copy-start.12 = (bf16[8,2,64,128]{3,0,1,2:T(8,128)(2,1)S(1)}, bf16[8,2,64,128]{3,0,1,2:T(8,128)(2,1)}, u32[]{:S(2)}) copy-start(bf16[8,2,64,128]{3,0,1,2:T(8,128)(2,1)} %get-tuple-element.190) | copy-start | bytes 786436
  144.0 79.2 %reduce-scatter.3.cloned.1.call-start = ((), (), s32[]{:S(2)}) async-start(), calls=%async_computation.2 | async-start | bytes 786432 | tf_op jit(solution)/shard_map/reduce_scatter | solution.py:109
  169.5 13.3 %copy-start.19 = (f32[1024]{0:T(1024)S(1)}, f32[1024]{0:T(1024)}, u32[]{:S(2)}) copy-start(f32[1024]{0:T(1024)} %param.28) | copy-start | bytes 12292
  182.6 4.3 %copy-start.2 = (bf16[128,2048]{1,0:T(8,128)(2,1)S(1)}, bf16[128,2048]{1,0:T(8,128)(2,1)}, u32[]{:S(2)}) copy-start(bf16[128,2048]{1,0:T(8,128)(2,1)} %copy-done.1) | copy-start | bytes 1572868
Sparse Core Ops, SparseCore 0:
  106.9 31.7 all-gather.4
  140.3 29.1 all-gather.6
  171.8 35.2 reduce-scatter.4
  209.7 13.3 reduce-scatter.2
